TPU v7x, 32 devices: a whole 2x2x4 slice. The times are simulated.
32 devices in a mesh: sp: 8 (over z, y), tp: 4 (over x, core).
Axes of the slice: x: 2, y: 2, z: 4, core: 2. Of those that a mesh axis runs over, the one named last changes fastest.
Arguments:
- tokens: bfloat16 [4096, 2048], P('sp'), may hold values from -6 to 6
- norm_gain: bfloat16 [2048], replicated, may hold values from 0.099609375 to 1.8984375
- w_conv_value: bfloat16 [2048, 2048], P('sp', 'tp'), may hold values from -0.125 to 0.125
- w_conv_gate: bfloat16 [2048, 2048], P('sp', 'tp'), may hold values from -0.125 to 0.125
- w_query: bfloat16 [2048, 2048], P('sp', 'tp'), may hold values from -0.125 to 0.125
- w_key: bfloat16 [2048, 512], P('sp', 'tp'), may hold values from -0.125 to 0.125
- w_value: bfloat16 [2048, 512], P('sp', 'tp'), may hold values from -0.125 to 0.125
- conv_taps: float32 [31, 2048], P(None, 'tp'), as said below
- ln_gain: float32 [2048], P('tp'), may hold values from 0.1 to 1.9
- sinks: float32 [32], P('tp'), may hold values from 3 to 6
- out_conv: bfloat16 [2048, 2048], P('tp', 'sp'), may hold values from -0.125 to 0.125
- out_attn: bfloat16 [2048, 2048], P('tp', 'sp'), may hold values from -0.5 to 0.5
Outputs:
- mixed: bfloat16 [4096, 2048], P(('sp', 'tp'))
- log_sums: float32 [32, 4096], P('tp', 'sp')
Inputs may be any that keep to these rules, and one draw needn't show every extreme that they name: `conv_taps`: each tap lies within 30 / sqrt(31) in magnitude.
All inputs are finite; a program needn't handle non-finite values.
Results may differ from a plain program's by a relative error of at most 0.017.
Values may be sent and summed in bfloat16 or wider, within the bound.
A program may use at most 64 MiB of HBM per device.

v0:
```python
import jax
import jax.numpy as jnp
from jax import lax
from jax.sharding import PartitionSpec as P

CONV_CH = 2048
HEADS = 32
KV_HEADS = 8
HEAD_DIM = 64
WINDOW = 128


NORM_EPS = 1e-06
CHANNEL_EPS = 1e-05
ROPE_BASE = 10000.0


def shifted(value, axis, steps):
    count = lax.axis_size(axis)
    initial, last = (max(0, -steps), min(count, count - steps))
    return lax.ppermute(value, axis, [(source, source + steps) for source in range(initial, last)])


def rotate(heads, positions):
    half_dim = heads.shape[-1] // 2
    inverse = ROPE_BASE ** (-jnp.arange(half_dim, dtype=jnp.float32) / half_dim)
    angles = positions.astype(jnp.float32)[:, None] * inverse[None, :]
    cosine = jnp.cos(angles)[:, None, :]
    sine = jnp.sin(angles)[:, None, :]
    as_float = heads.astype(jnp.float32)
    front_part = as_float[..., :half_dim]
    back_part = as_float[..., half_dim:]
    return jnp.concatenate(
        [front_part * cosine - back_part * sine, back_part * cosine + front_part * sine], axis=-1
    )


def shards(
    tokens,
    norm_gain,
    w_conv_value,
    w_conv_gate,
    w_query,
    w_key,
    w_value,
    conv_taps,
    ln_gain,
    sinks,
    out_conv,
    out_attn,
):
    as_float = tokens.astype(jnp.float32)
    normed = (
        as_float
        * lax.rsqrt(jnp.mean(as_float * as_float, axis=-1, keepdims=True) + NORM_EPS)
        * norm_gain.astype(jnp.float32)
    ).astype(jnp.bfloat16)
    row_count = normed.shape[0]
    pieces = (
        lax.all_gather(w_conv_value, "sp", axis=0, tiled=True),
        lax.all_gather(w_conv_gate, "sp", axis=0, tiled=True),
        lax.all_gather(w_query, "sp", axis=0, tiled=True),
        lax.all_gather(w_key, "sp", axis=0, tiled=True),
        lax.all_gather(w_value, "sp", axis=0, tiled=True),
    )
    projected = tuple(
        (jnp.dot(normed, piece, preferred_element_type=jnp.float32) for piece in pieces)
    )
    conv_value, conv_gate, query_raw, key_raw, value_rows = [
        item.astype(jnp.bfloat16) for item in projected
    ]
    glu = (conv_value.astype(jnp.float32) * jax.nn.sigmoid(conv_gate.astype(jnp.float32))).astype(
        jnp.bfloat16
    )
    offset = lax.axis_index("sp") * row_count
    positions = offset + jnp.arange(row_count, dtype=jnp.int32)
    query_heads = query_raw.shape[1] // HEAD_DIM
    key_heads = key_raw.shape[1] // HEAD_DIM
    query = rotate(query_raw.reshape(row_count, query_heads, HEAD_DIM), positions).astype(
        jnp.bfloat16
    )
    key = rotate(key_raw.reshape(row_count, key_heads, HEAD_DIM), positions).astype(jnp.bfloat16)
    reach = conv_taps.shape[0] - 1
    key_tail = key[row_count - WINDOW :]
    value_tail = value_rows.reshape(row_count, key_heads, HEAD_DIM)[row_count - WINDOW :]
    glu_tail = glu[row_count - reach :]
    glu_before = shifted(glu_tail, "sp", 1)
    key_before, value_before = shifted((key_tail, value_tail), "sp", 1)
    extended = jnp.concatenate([glu_before, glu], axis=0).astype(jnp.float32)
    conv_out = jnp.zeros((row_count, glu.shape[1]), jnp.float32)
    for tap in range(reach + 1):
        conv_out = conv_out + conv_taps[tap][None, :] * extended[tap : tap + row_count]
    sum_first = jnp.sum(conv_out, axis=-1)
    sum_second = jnp.sum(conv_out * conv_out, axis=-1)
    total_first, total_second = lax.psum((sum_first, sum_second), "tp")
    mean = (total_first / CONV_CH)[:, None]
    var = (total_second / CONV_CH)[:, None] - mean * mean
    conv_branch = jax.nn.silu(
        (conv_out - mean) * lax.rsqrt(var + CHANNEL_EPS) * ln_gain[None, :]
    ).astype(jnp.bfloat16)
    group = HEADS // KV_HEADS
    blocks = row_count // WINDOW
    q_blocks = query.reshape(blocks, WINDOW, key_heads, group, HEAD_DIM)
    key_blocks = jnp.concatenate([key_before, key], axis=0).reshape(
        blocks + 1, WINDOW, key_heads, HEAD_DIM
    )
    value_all = jnp.concatenate(
        [value_before, value_rows.reshape(row_count, key_heads, HEAD_DIM)], axis=0
    )
    value_blocks = value_all.reshape(blocks + 1, WINDOW, key_heads, HEAD_DIM)
    key_window = jnp.concatenate([key_blocks[:-1], key_blocks[1:]], axis=1)
    value_window = jnp.concatenate([value_blocks[:-1], value_blocks[1:]], axis=1)
    scores = jnp.einsum(
        "nqhgd,nkhd->nhgqk", q_blocks, key_window, preferred_element_type=jnp.float32
    ) * HEAD_DIM ** (-0.5)
    query_index = jnp.arange(WINDOW)[:, None] + WINDOW
    key_index = jnp.arange(2 * WINDOW)[None, :]
    band = (key_index <= query_index) & (query_index - key_index < WINDOW)
    block_index = jnp.arange(blocks)[:, None, None]
    allowed = band[None] & (offset + block_index * WINDOW + key_index[None] - WINDOW >= 0)
    allowed = allowed[:, None, None]
    totals = jnp.sum(jnp.where(allowed, jnp.exp(scores), 0.0), axis=-1)
    totals = totals + jnp.exp(sinks).reshape(1, key_heads, group, 1)
    log_total = jnp.log(totals)
    weights = jnp.where(allowed, jnp.exp(scores - log_total[..., None]), 0.0).astype(jnp.bfloat16)
    attended = jnp.einsum(
        "nhgqk,nkhd->nqhgd", weights, value_window, preferred_element_type=jnp.float32
    )
    attn_branch = attended.astype(jnp.bfloat16).reshape(row_count, query_heads * HEAD_DIM)
    log_sums = log_total.transpose(1, 2, 0, 3).reshape(query_heads, row_count)
    cols_conv, cols_attn = (
        lax.all_gather(out_conv, "sp", axis=1, tiled=True),
        lax.all_gather(out_attn, "sp", axis=1, tiled=True),
    )
    mixed = lax.psum_scatter(
        (
            jnp.dot(conv_branch, cols_conv, preferred_element_type=jnp.float32)
            + jnp.dot(attn_branch, cols_attn, preferred_element_type=jnp.float32)
        ).astype(jnp.bfloat16),
        "tp",
        scatter_dimension=0,
        tiled=True,
    )
    return (mixed, log_sums)


def solution(mesh):
    in_specs = (
        P("sp", None),
        P(),
        P("sp", "tp"),
        P("sp", "tp"),
        P("sp", "tp"),
        P("sp", "tp"),
        P("sp", "tp"),
        P(None, "tp"),
        P("tp"),
        P("tp"),
        P("tp", "sp"),
        P("tp", "sp"),
    )
    out_specs = (P(("sp", "tp"), None), P("tp", "sp"))
    return jax.shard_map(shards, mesh=mesh, in_specs=in_specs, out_specs=out_specs, check_vma=False)
```

profile of v0, /device:TPU:0, one launch (start us, length us, event | category | flops | bytes accessed | tf_op | source)
XLA Modules:
  0.0 311.6 jit_solution(11297388451167139868)
XLA Ops:
  8.0 0.7 all-gather.6.cloned.1.call-update
  10.0 0.7 convert_element_type.76
  10.7 2.1 fusion
  12.8 34.2 %all_gather.25 = bf16[2048,128]{1,0:T(8,128)(2,1)S(1)} all-gather(bf16[256,128]{1,0:T(8,128)(2,1)S(1)} %copy-done.1), channel_id=1, replica_groups=mesh['sp'=8,'tp'=4] {'sp'}, dimensions={0}, use_global_device_ids=true | all-gather | bytes 589824 | tf_op jit(solution)/shard_map/all_gather | solution.py:63
  47.0 0.9 convolution_convert_fusion.3
  48.4 3.7 %collective-permute-start.2 = (bf16[128,2,64]{0,2,1:T(8,128)(2,1)S(1)}, bf16[128,2,64]{0,2,1:T(8,128)(2,1)S(1)}, u32[]{:S(2)}, u32[]{:S(2)}) collective-permute-start(bf16[128,2,64]{0,2,1:T(8,128)(2,1)S(1)} %pad_maximum_fusion.3), channel_id=1, source_target_pairs={{0,4},{4,8},{8,12},{12,16},{16,20},{20,24},{24,28},{1,5},{5,9},{9,... | collective-permute-start | bytes 98312 | tf_op jit(solution)/shard_map/ppermute | solution.py:21
  52.2 32.8 %all_gather.24 = bf16[2048,128]{1,0:T(8,128)(2,1)S(1)} all-gather(bf16[256,128]{1,0:T(8,128)(2,1)S(1)} %copy-done.2), channel_id=1, replica_groups=mesh['sp'=8,'tp'=4] {'sp'}, dimensions={0}, use_global_device_ids=true | all-gather | bytes 589824 | tf_op jit(solution)/shard_map/all_gather | solution.py:64
  84.9 0.9 convolution_convert_fusion.4
  85.9 1.3 collective-permute-start.1
  90.5 3.0 convolution_convert_fusion
  94.0 24.7 %all-gather.6.cloned.1.call-done = bf16[2048,512]{1,0:T(8,128)(2,1)} async-done(((bf16[256,512]{1,0:T(8,128)(2,1)}), bf16[2048,512]{1,0:T(8,128)(2,1)}) %all-gather.6.cloned.1.call-update) | async-done | bytes 2097168 | tf_op jit(solution)/shard_map/all_gather | solution.py:60
  118.8 3.8 %fusion.21 = f32[512,512]{1,0:T(8,128)} fusion(bf16[2048,512]{1,0:T(8,128)(2,1)} %all-gather.6.cloned.1.call-done, bf16[512,2048]{1,0:T(8,128)(2,1)S(1)} %copy-done, f32[2048]{0:T(1024)S(1)} %copy-done.35, f32[512]{0:T(512)S(1)} %copy-done.38), kind=kOutput, calls=%fused_computation.28 | convolution fusion | flops 1078460416 | bytes 5253120 | tf_op jit(solution)/shard_map/dot_general | solution.py:67
  122.6 45.9 %all-gather.8.cloned.1.call-done = bf16[2048,512]{1,0:T(8,128)(2,1)} async-done(((bf16[256,512]{1,0:T(8,128)(2,1)}), bf16[2048,512]{1,0:T(8,128)(2,1)}) %all-gather.8.cloned.1.call-update) | async-done | bytes 2097168 | tf_op jit(solution)/shard_map/all_gather | solution.py:61
  168.5 3.3 %fusion.20 = bf16[512,512]{1,0:T(8,128)(2,1)S(1)} fusion(f32[512,512]{1,0:T(8,128)} %fusion.21, bf16[2048,512]{1,0:T(8,128)(2,1)} %all-gather.8.cloned.1.call-done, bf16[512,2048]{1,0:T(8,128)(2,1)S(1)} %copy-done, f32[2048]{0:T(1024)S(1)} %copy-done.36, f32[512]{0:T(512)S(1)} %copy-done.39), kind=kOutput, calls=%fused_computation.26 | convolution fusion | flops 1079771136 | bytes 5777408 | tf_op jit(solution)/shard_map/dot_general | solution.py:67
  171.9 2.6 collective-permute-start
  174.5 1.1 fusion.4
  175.8 0.9 fusion.25
  177.8 5.1 %fusion.88 = (f32[512]{0:T(512)S(1)}, f32[512]{0:T(512)S(1)}, f32[512,512]{1,0:T(8,128)S(1)}) fusion(f32[542,512]{1,0:T(8,128)S(1)} %maximum_convert_fusion, f32[512]{0:T(512)S(1)} %bitcast.147, f32[512]{0:T(512)S(1)} %bitcast.148, f32[512]{0:T(512)S(1)} %bitcast.119, f32[512]{0:T(512)S(1)} %bitcast.120, f32[512]{0:T(512)S(1)} %bitcast.121, ...), kind=kLoop, calls=%fused_computation.150 | loop fusion | flops 16776192 | bytes 33622016 | tf_op jit(solution)/shard_map/reduce_sum | solution.py:93
  182.9 6.1 %all-reduce = (f32[512]{0:T(512)S(1)}, f32[512]{0:T(512)S(1)}) all-reduce(f32[512]{0:T(512)S(1)} %get-tuple-element.3, f32[512]{0:T(512)S(1)} %get-tuple-element.2), channel_id=1, replica_groups=mesh['sp'=8,'tp'=4] {'tp'}, use_global_device_ids=true, to_apply=%region_4.0 | all-reduce | flops 1024 | bytes 8192 | tf_op jit(solution)/shard_map/psum | solution.py:95
  189.0 30.3 %all-gather.10.cloned.1.call-done = bf16[512,2048]{1,0:T(8,128)(2,1)} async-done(((bf16[512,256]{1,0:T(8,128)(2,1)}), bf16[512,2048]{1,0:T(8,128)(2,1)}) %all-gather.10.cloned.1.call-update) | async-done | bytes 2097168 | tf_op jit(solution)/shard_map/all_gather | solution.py:132
  219.3 5.0 %fusion.58 = f32[512,2048]{1,0:T(8,128)} fusion(bf16[512,2048]{1,0:T(8,128)(2,1)} %all-gather.10.cloned.1.call-done, f32[512,512]{1,0:T(8,128)S(1)} %get-tuple-element.6, f32[512]{0:T(512)S(1)} %copy-done.41, f32[512]{0:T(512)S(1)} %get-tuple-element.45, f32[512]{0:T(512)S(1)} %get-tuple-element.44), kind=kOutput, calls=%fused_computation.97 | convolution fusion | flops 1075838976 | bytes 7346176 | tf_op jit(solution)/shard_map/dot_general | solution.py:137
  224.4 45.4 %all-gather.14.cloned.1.call-done = bf16[512,2048]{1,0:T(8,128)(2,1)} async-done(((bf16[512,256]{1,0:T(8,128)(2,1)}), bf16[512,2048]{1,0:T(8,128)(2,1)}) %all-gather.14.cloned.1.call-update) | async-done | bytes 2097168 | tf_op jit(solution)/shard_map/all_gather | solution.py:133
  269.8 5.5 %add_convert_fusion = bf16[512,2048]{1,0:T(8,128)(2,1)} fusion(f32[512,2048]{1,0:T(8,128)} %fusion.58, bf16[512,2048]{1,0:T(8,128)(2,1)} %all-gather.14.cloned.1.call-done, bf16[64,8,4,128]{3,2,1,0:T(4,128)(2,1)S(1)} %bitcast.112), kind=kOutput, calls=%fused_computation.12 | convolution fusion | flops 1075838976 | bytes 8912896 | tf_op jit(solution)/shard_map/dot_general | solution.py:138
  275.3 29.5 %reduce-scatter.2.cloned.1.call-done = bf16[128,2048]{1,0:T(8,128)(2,1)} async-done(((bf16[512,2048]{1,0:T(8,128)(2,1)}), bf16[128,2048]{1,0:T(8,128)(2,1)}) %reduce-scatter.2.cloned.1.call-update) | async-done | bytes 524304 | tf_op jit(solution)/shard_map/reduce_scatter | solution.py:135
  (134 shorter events, 7.0 us)
Async XLA Ops:
  7.2 39.9 %copy-start = (bf16[512,2048]{1,0:T(8,128)(2,1)S(1)}, bf16[512,2048]{1,0:T(8,128)(2,1)}, u32[]{:S(2)}) copy-start(bf16[512,2048]{1,0:T(8,128)(2,1)} %param.12) | copy-start | bytes 6291460
  7.2 5.6 %copy-start.1 = (bf16[256,128]{1,0:T(8,128)(2,1)S(1)}, bf16[256,128]{1,0:T(8,128)(2,1)}, u32[]{:S(2)}) copy-start(bf16[256,128]{1,0:T(8,128)(2,1)} %param.17) | copy-start | bytes 196612
  7.2 83.3 %all-gather.12.cloned.1.call-start = ((), (), s32[]{:S(2)}) async-start(), calls=%async_computation.4 | async-start | bytes 2359296 | tf_op jit(solution)/shard_map/all_gather | solution.py:62
  7.9 110.8 %all-gather.6.cloned.1.call-start = ((), (), s32[]{:S(2)}) async-start(), calls=%async_computation.1 | async-start | bytes 2359296 | tf_op jit(solution)/shard_map/all_gather | solution.py:60
  8.7 159.9 %all-gather.8.cloned.1.call-start = ((), (), s32[]{:S(2)}) async-start(), calls=%async_computation.2 | async-start | bytes 2359296 | tf_op jit(solution)/shard_map/all_gather | solution.py:61
  9.4 209.9 %all-gather.10.cloned.1.call-start = ((), (), s32[]{:S(2)}) async-start(), calls=%async_computation.3 | async-start | bytes 2359296 | tf_op jit(solution)/shard_map/all_gather | solution.py:132
  10.0 259.8 %all-gather.14.cloned.1.call-start = ((), (), s32[]{:S(2)}) async-start(), calls=%async_computation.5 | async-start | bytes 2359296 | tf_op jit(solution)/shard_map/all_gather | solution.py:133
  10.7 79.7 %copy-start.34 = (f32[2048]{0:T(1024)}, f32[2048]{0:T(1024)S(1)}, u32[]{:S(2)}) copy-start(f32[2048]{0:T(1024)S(1)} %convert_element_type.76) | copy-start | bytes 24580
  12.8 77.6 %copy-start.37 = (f32[512]{0:T(512)}, f32[512]{0:T(512)S(1)}, u32[]{:S(2)}) copy-start(f32[512]{0:T(512)S(1)} %add_rsqrt_fusion.1) | copy-start | bytes 6148
  47.0 5.1 %copy-start.2 = (bf16[256,128]{1,0:T(8,128)(2,1)S(1)}, bf16[256,128]{1,0:T(8,128)(2,1)}, u32[]{:S(2)}) copy-start(bf16[256,128]{1,0:T(8,128)(2,1)} %param.18) | copy-start | bytes 196612
  48.4 41.9 %collective-permute-start.2 = (bf16[128,2,64]{0,2,1:T(8,128)(2,1)S(1)}, bf16[128,2,64]{0,2,1:T(8,128)(2,1)S(1)}, u32[]{:S(2)}, u32[]{:S(2)}) collective-permute-start(bf16[128,2,64]{0,2,1:T(8,128)(2,1)S(1)} %pad_maximum_fusion.3), channel_id=1, source_target_pairs={{0,4},{4,8},{8,12},{12,16},{16,20},{20,24},{24,28},{1,5},{5,9},{9,... | collective-permute-start | bytes 98312 | tf_op jit(solution)/shard_map/ppermute | solution.py:21
  84.9 3.1 %copy-start.5 = (f32[31,512]{1,0:T(8,128)S(1)}, f32[31,512]{1,0:T(8,128)}, u32[]{:S(2)}) copy-start(f32[31,512]{1,0:T(8,128)} %param.19) | copy-start | bytes 190468
  84.9 4.7 %copy-start.42 = (f32[8]{0:T(128)S(1)}, f32[8]{0:T(128)}, u32[]{:S(2)}) copy-start(f32[8]{0:T(128)} %param.21) | copy-start | bytes 100
  85.9 4.5 %collective-permute-start.1 = (bf16[128,2,64]{0,2,1:T(8,128)(2,1)S(1)}, bf16[128,2,64]{0,2,1:T(8,128)(2,1)S(1)}, u32[]{:S(2)}, u32[]{:S(2)}) collective-permute-start(bf16[128,2,64]{0,2,1:T(8,128)(2,1)S(1)} %bitcast.116), channel_id=1, source_target_pairs={{0,4},{4,8},{8,12},{12,16},{16,20},{20,24},{24,28},{1,5},{5,9},{9,... | collective-permute-start | bytes 98312 | tf_op jit(solution)/shard_map/ppermute | solution.py:21
  87.2 217.6 %reduce-scatter.2.cloned.1.call-start = ((), (), s32[]{:S(2)}) async-start(), calls=%async_computation.6 | async-start | bytes 2621440 | tf_op jit(solution)/shard_map/reduce_scatter | solution.py:135
  93.7 25.0 %copy-start.35 = (f32[2048]{0:T(1024)S(1)}, f32[2048]{0:T(1024)}, u32[]{:S(2)}) copy-start(f32[2048]{0:T(1024)} %copy-done.34) | copy-start | bytes 24580
  93.8 25.0 %copy-start.38 = (f32[512]{0:T(512)S(1)}, f32[512]{0:T(512)}, u32[]{:S(2)}) copy-start(f32[512]{0:T(512)} %copy-done.37) | copy-start | bytes 6148
  94.0 74.5 %copy-start.36 = (f32[2048]{0:T(1024)S(1)}, f32[2048]{0:T(1024)}, u32[]{:S(2)}) copy-start(f32[2048]{0:T(1024)} %copy-done.34) | copy-start | bytes 24580
  94.0 74.5 %copy-start.39 = (f32[512]{0:T(512)S(1)}, f32[512]{0:T(512)}, u32[]{:S(2)}) copy-start(f32[512]{0:T(512)} %copy-done.37) | copy-start | bytes 6148
  122.6 51.9 %copy-start.3 = (bf16[4,128,2,32]{1,3,2,0:T(8,128)(2,1)S(1)}, bf16[4,128,2,32]{1,3,2,0:T(8,128)(2,1)}, u32[]{:S(2)}) copy-start(bf16[4,128,2,32]{1,3,2,0:T(8,128)(2,1)} %get-tuple-element.48) | copy-start | bytes 196612
  122.6 51.9 %copy-start.4 = (bf16[4,128,2,32]{1,3,2,0:T(8,128)(2,1)S(1)}, bf16[4,128,2,32]{1,3,2,0:T(8,128)(2,1)}, u32[]{:S(2)}) copy-start(bf16[4,128,2,32]{1,3,2,0:T(8,128)(2,1)} %get-tuple-element.49) | copy-start | bytes 196612
  171.9 5.5 %collective-permute-start = (bf16[30,512]{1,0:T(8,128)(2,1)S(1)}, bf16[30,512]{1,0:T(8,128)(2,1)S(1)}, u32[]{:S(2)}, u32[]{:S(2)}) collective-permute-start(bf16[30,512]{1,0:T(8,128)(2,1)S(1)} %slice.303), channel_id=1, source_target_pairs={{0,4},{4,8},{8,12},{12,16},{16,20},{20,24},{24,28},{1,5},{5,9},{9,... | collective-permute-start | bytes 92168 | tf_op jit(solution)/shard_map/ppermute | solution.py:21
  174.5 1.1 copy-start.40
  177.8 41.5 %copy-start.41 = (f32[512]{0:T(512)S(1)}, f32[512]{0:T(512)}, u32[]{:S(2)}) copy-start(f32[512]{0:T(512)} %param.20) | copy-start | bytes 6148
  (28 other events, 24.3 us)
Sparse Core Ops, SparseCore 0:
  10.1 57.5 all-gather.11
  69.9 48.8 all-gather.5
  120.9 47.6 all-gather.7
  170.4 48.8 all-gather.9
  221.2 48.5 all-gather.13
  275.4 29.3 reduce-scatter.1
where the time goes:
time: 312 us
  waiting for transfers between devices  179 us (57%)
  blocking collectives  73 us (23%)
  matrix products  24.5 us (8%)
  between operations  14.9 us (5%)
  other arithmetic  9.14 us (3%)
  starting transfers between devices  7.91 us (3%)
  local copies, waits for them, and re-layouts  3.55 us (1%)
    all_gather x1, waiting for transfers between devices, shards(): lax.all_gather(w_conv_gate, 'sp', axis=0, tiled=True)  45.9 us
    all_gather x1, waiting for transfers between devices, shards(): lax.all_gather(out_attn, 'sp', axis=1, tiled=True)  45.4 us
    all_gather x1, blocking collectives, shards(): lax.all_gather(w_key, 'sp', axis=0, tiled=True)  34.2 us
    all_gather x1, blocking collectives, shards(): lax.all_gather(w_value, 'sp', axis=0, tiled=True)  32.8 us
    all_gather x1, waiting for transfers between devices, shards(): lax.all_gather(out_conv, 'sp', axis=1, tiled=True)  30.3 us
    reduce_scatter x1, waiting for transfers between devices, shards(): lax.psum_scatter((jnp.dot(conv_branch, cols_conv, preferred_element_type=...  29.5 us
    all_gather x1, waiting for transfers between devices, shards(): lax.all_gather(w_conv_value, 'sp', axis=0, tiled=True)  24.7 us
    dot_general x5, matrix products, shards(): jnp.dot(normed, piece, preferred_element_type=jnp.float32)  12 us
  transfers between devices with their start and end apart: 9, of which 5 were waited for; matrix products, arithmetic and copies ran while one was open for 10% of the time, Pallas kernels for 0%

commit v1 on v0

--- a/solution.py
+++ b/solution.py
@@ -1,6 +1,10 @@
+import functools
+
 import jax
 import jax.numpy as jnp
 from jax import lax
+from jax.experimental import pallas as pl
+from jax.experimental.pallas import tpu as pltpu
 from jax.sharding import PartitionSpec as P
 
 CONV_CH = 2048
@@ -33,6 +37,295 @@
     return jnp.concatenate(
         [front_part * cosine - back_part * sine, back_part * cosine + front_part * sine], axis=-1
     )
+
+
+def ring_place(index, count):
+    half = count // 2
+    index = lax.rem(index + 2 * count, count)
+    return jnp.where(index < half, 2 * index, 2 * (count - 1 - index) + 1)
+
+
+class Ring:
+    def __init__(self, count, phases, send_sem, recv_sem):
+        self.count, self.phases = count, phases
+        self.send_sem, self.recv_sem = send_sem, recv_sem
+        me = lax.axis_index("sp")
+        half = count // 2
+        spot = jnp.where(lax.rem(me, 2) == 0, me // 2, count - 1 - me // 2)
+        self.spot = spot
+        self.peers = (ring_place(spot + 1, count), ring_place(spot - 1, count))
+
+    def owner(self, way, step):
+        return ring_place(self.spot - step if way == 0 else self.spot + step, self.count)
+
+    def copy(self, phase, way, piece, step):
+        own, place = self.phases[phase][way][piece]
+        target = place(self.owner(way, step))
+        number = sum(len(p[0]) for p in self.phases[:phase]) + piece
+        return pltpu.make_async_remote_copy(
+            src_ref=own if step == 0 else target,
+            dst_ref=target,
+            send_sem=self.send_sem.at[way, number, step],
+            recv_sem=self.recv_sem.at[way, number, step],
+            device_id={"sp": self.peers[way]},
+            device_id_type=pl.DeviceIdType.MESH,
+        )
+
+    def arrived(self, phase, way, piece, step):
+        own, place = self.phases[phase][way][piece]
+        target = place(self.owner(way, step + 1))
+        number = sum(len(p[0]) for p in self.phases[:phase]) + piece
+        pltpu.make_async_remote_copy(
+            src_ref=target,
+            dst_ref=target,
+            send_sem=self.send_sem.at[way, number, step],
+            recv_sem=self.recv_sem.at[way, number, step],
+            device_id={"sp": self.peers[way]},
+            device_id_type=pl.DeviceIdType.MESH,
+        ).wait_recv()
+
+    def begin(self, phase):
+        for piece in range(len(self.phases[phase][0])):
+            for way in range(2):
+                self.copy(phase, way, piece, 0).start()
+
+    def advance(self, phase, step):
+        for piece in range(len(self.phases[phase][0])):
+            for way in range(2):
+                self.arrived(phase, way, piece, step)
+                if step + 1 < self.count - 1:
+                    self.copy(phase, way, piece, step + 1).start()
+
+    def drain(self):
+        for phase in range(len(self.phases)):
+            for piece in range(len(self.phases[phase][0])):
+                for way in range(2):
+                    for step in range(self.count - 1):
+                        self.copy(phase, way, piece, step).wait_send()
+
+
+def run_phase(ring, phase, work):
+    steps = ring.count - 1
+    done = 0
+    for step in range(steps):
+        upto = (step + 1) * len(work) // steps
+        for item in work[done:upto]:
+            item()
+        done = upto
+        ring.advance(phase, step)
+        if step == steps - 2 and phase + 1 < len(ring.phases):
+            ring.begin(phase + 1)
+
+
+def gather_kernel(
+    count,
+    tokens,
+    norm_gain,
+    w_conv_value,
+    w_conv_gate,
+    w_query,
+    w_key,
+    w_value,
+    out_conv,
+    out_attn,
+    glu_out,
+    query_out,
+    key_out,
+    value_out,
+    full_conv,
+    full_attn,
+    normed,
+    full_cv,
+    full_cg,
+    full_q,
+    full_k,
+    full_v,
+    send_sem,
+    recv_sem,
+    own_sem,
+):
+    me = lax.axis_index("sp")
+    depth, wide = w_query.shape
+    narrow = w_key.shape[1]
+    long, cols = out_conv.shape
+    rows = tokens.shape[0]
+
+    def by_rows(own, full, low, high):
+        return (
+            own.at[:, pl.ds(low, high - low)],
+            lambda who: full.at[
+                pl.ds(pl.multiple_of(who * depth, depth), depth), pl.ds(low, high - low)
+            ],
+        )
+
+    def by_cols(own, full, low, high):
+        return (
+            own.at[pl.ds(low, high - low)],
+            lambda who: full.at[
+                pl.ds(low, high - low), pl.ds(pl.multiple_of(who * cols, cols), cols)
+            ],
+        )
+
+    quarter, middle = wide // 4, wide // 2
+    phases = (
+        (
+            [by_rows(w_query, full_q, i * quarter, (i + 1) * quarter) for i in range(3)],
+            [
+                by_rows(w_query, full_q, 3 * quarter, wide),
+                by_rows(w_key, full_k, 0, narrow),
+                by_rows(w_value, full_v, 0, narrow),
+            ],
+        ),
+        (
+            [by_rows(w_conv_value, full_cv, i * middle, (i + 1) * middle) for i in range(2)],
+            [by_rows(w_conv_gate, full_cg, i * middle, (i + 1) * middle) for i in range(2)],
+        ),
+        (
+            [by_cols(out_conv, full_conv, i * long // 2, (i + 1) * long // 2) for i in range(2)],
+            [by_cols(out_attn, full_attn, i * long // 2, (i + 1) * long // 2) for i in range(2)],
+        ),
+    )
+    ring = Ring(count, phases, send_sem, recv_sem)
+    barrier = pltpu.get_barrier_semaphore()
+    for peer in ring.peers:
+        pl.semaphore_signal(
+            barrier, inc=1, device_id={"sp": peer}, device_id_type=pl.DeviceIdType.MESH
+        )
+    pl.semaphore_wait(barrier, 2)
+    ring.begin(0)
+
+    mine = pl.ds(pl.multiple_of(me * depth, depth), depth)
+    my_cols = pl.ds(pl.multiple_of(me * cols, cols), cols)
+    local = [
+        pltpu.make_async_copy(own, place, own_sem.at[i])
+        for i, (own, place) in enumerate(
+            (
+                (w_conv_value, full_cv.at[mine]),
+                (w_conv_gate, full_cg.at[mine]),
+                (w_query, full_q.at[mine]),
+                (w_key, full_k.at[mine]),
+                (w_value, full_v.at[mine]),
+                (out_conv, full_conv.at[:, my_cols]),
+                (out_attn, full_attn.at[:, my_cols]),
+            )
+        )
+    ]
+    for item in local:
+        item.start()
+
+    def norm(part):
+        take = pl.ds(part * 64, 64)
+        x = tokens[take, :].astype(jnp.float32)
+        scale = lax.rsqrt(jnp.mean(x * x, axis=-1, keepdims=True) + NORM_EPS)
+        normed[take, :] = (x * scale * norm_gain[...].astype(jnp.float32)).astype(jnp.bfloat16)
+
+    def product(take, full):
+        return jnp.dot(normed[take, :], full[...], preferred_element_type=jnp.float32).astype(
+            jnp.bfloat16
+        )
+
+    def attention_side(part):
+        take = pl.ds(part * 128, 128)
+        query_out[take, :] = product(take, full_q)
+        key_out[take, :] = product(take, full_k)
+        value_out[take, :] = product(take, full_v)
+
+    def conv_side(part):
+        take = pl.ds(part * 128, 128)
+        value = product(take, full_cv).astype(jnp.float32)
+        gate = product(take, full_cg).astype(jnp.float32)
+        glu_out[take, :] = (value * jax.nn.sigmoid(gate)).astype(jnp.bfloat16)
+
+    run_phase(ring, 0, [functools.partial(norm, i) for i in range(rows // 64)])
+    for item in local:
+        item.wait()
+    run_phase(ring, 1, [functools.partial(attention_side, i) for i in range(rows // 128)])
+    run_phase(ring, 2, [functools.partial(conv_side, i) for i in range(rows // 128)])
+    ring.drain()
+
+
+def fits(count, shape_in, shape_out, rows):
+    tiled = shape_in[0] % 128 == 0 and shape_in[1] % 512 == 0 and shape_out[1] % 128 == 0
+    return tiled and rows % 128 == 0 and count % 2 == 0 and count > 3
+
+
+def gathered(
+    tokens, norm_gain, w_conv_value, w_conv_gate, w_query, w_key, w_value, out_conv, out_attn
+):
+    count = lax.axis_size("sp")
+    rows, width = tokens.shape
+    wide, narrow = w_query.shape[1], w_key.shape[1]
+    long = out_conv.shape[0]
+    vmem = pl.BlockSpec(memory_space=pltpu.VMEM)
+    shape = lambda *dims: jax.ShapeDtypeStruct(dims, jnp.bfloat16)
+    scratch = lambda *dims: pltpu.VMEM(dims, jnp.bfloat16)
+    pieces = 7
+    return pl.pallas_call(
+        functools.partial(gather_kernel, count),
+        out_shape=(
+            shape(rows, w_conv_value.shape[1]),
+            shape(rows, wide),
+            shape(rows, narrow),
+            shape(rows, narrow),
+            shape(long, count * out_conv.shape[1]),
+            shape(out_attn.shape[0], count * out_attn.shape[1]),
+        ),
+        in_specs=[vmem] * 9,
+        out_specs=(vmem,) * 6,
+        scratch_shapes=[
+            scratch(rows, width),
+            scratch(width, w_conv_value.shape[1]),
+            scratch(width, w_conv_gate.shape[1]),
+            scratch(width, wide),
+            scratch(width, narrow),
+            scratch(width, narrow),
+            pltpu.SemaphoreType.DMA((2, pieces, count - 1)),
+            pltpu.SemaphoreType.DMA((2, pieces, count - 1)),
+            pltpu.SemaphoreType.DMA((7,)),
+        ],
+        compiler_params=pltpu.CompilerParams(collective_id=0, has_side_effects=True),
+        name="gather_project",
+    )(
+        tokens,
+        norm_gain.reshape(1, width),
+        w_conv_value,
+        w_conv_gate,
+        w_query,
+        w_key,
+        w_value,
+        out_conv,
+        out_attn,
+    )
+
+
+def plain(tokens, norm_gain, w_conv_value, w_conv_gate, w_query, w_key, w_value, out_conv, out_attn):
+    as_float = tokens.astype(jnp.float32)
+    normed = (
+        as_float
+        * lax.rsqrt(jnp.mean(as_float * as_float, axis=-1, keepdims=True) + NORM_EPS)
+        * norm_gain.astype(jnp.float32)
+    ).astype(jnp.bfloat16)
+    pieces = (
+        lax.all_gather(w_conv_value, "sp", axis=0, tiled=True),
+        lax.all_gather(w_conv_gate, "sp", axis=0, tiled=True),
+        lax.all_gather(w_query, "sp", axis=0, tiled=True),
+        lax.all_gather(w_key, "sp", axis=0, tiled=True),
+        lax.all_gather(w_value, "sp", axis=0, tiled=True),
+    )
+    projected = tuple(
+        (jnp.dot(normed, piece, preferred_element_type=jnp.float32) for piece in pieces)
+    )
+    conv_value, conv_gate, query_raw, key_raw, value_rows = [
+        item.astype(jnp.bfloat16) for item in projected
+    ]
+    glu = (conv_value.astype(jnp.float32) * jax.nn.sigmoid(conv_gate.astype(jnp.float32))).astype(
+        jnp.bfloat16
+    )
+    cols_conv, cols_attn = (
+        lax.all_gather(out_conv, "sp", axis=1, tiled=True),
+        lax.all_gather(out_attn, "sp", axis=1, tiled=True),
+    )
+    return glu, query_raw, key_raw, value_rows, cols_conv, cols_attn
 
 
 def shards(
@@ -49,28 +342,10 @@
     out_conv,
     out_attn,
 ):
-    as_float = tokens.astype(jnp.float32)
-    normed = (
-        as_float
-        * lax.rsqrt(jnp.mean(as_float * as_float, axis=-1, keepdims=True) + NORM_EPS)
-        * norm_gain.astype(jnp.float32)
-    ).astype(jnp.bfloat16)
-    row_count = normed.shape[0]
-    pieces = (
-        lax.all_gather(w_conv_value, "sp", axis=0, tiled=True),
-        lax.all_gather(w_conv_gate, "sp", axis=0, tiled=True),
-        lax.all_gather(w_query, "sp", axis=0, tiled=True),
-        lax.all_gather(w_key, "sp", axis=0, tiled=True),
-        lax.all_gather(w_value, "sp", axis=0, tiled=True),
-    )
-    projected = tuple(
-        (jnp.dot(normed, piece, preferred_element_type=jnp.float32) for piece in pieces)
-    )
-    conv_value, conv_gate, query_raw, key_raw, value_rows = [
-        item.astype(jnp.bfloat16) for item in projected
-    ]
-    glu = (conv_value.astype(jnp.float32) * jax.nn.sigmoid(conv_gate.astype(jnp.float32))).astype(
-        jnp.bfloat16
+    row_count = tokens.shape[0]
+    whole = fits(lax.axis_size("sp"), w_query.shape, out_conv.shape, row_count)
+    glu, query_raw, key_raw, value_rows, cols_conv, cols_attn = (gathered if whole else plain)(
+        tokens, norm_gain, w_conv_value, w_conv_gate, w_query, w_key, w_value, out_conv, out_attn
     )
     offset = lax.axis_index("sp") * row_count
     positions = offset + jnp.arange(row_count, dtype=jnp.int32)
@@ -128,10 +403,6 @@
     )
     attn_branch = attended.astype(jnp.bfloat16).reshape(row_count, query_heads * HEAD_DIM)
     log_sums = log_total.transpose(1, 2, 0, 3).reshape(query_heads, row_count)
-    cols_conv, cols_attn = (
-        lax.all_gather(out_conv, "sp", axis=1, tiled=True),
-        lax.all_gather(out_attn, "sp", axis=1, tiled=True),
-    )
     mixed = lax.psum_scatter(
         (
             jnp.dot(conv_branch, cols_conv, preferred_element_type=jnp.float32)

time: 312 us -> 201 us (0.64)
  waiting for transfers between devices: 179 us -> 30.4 us
  Pallas kernels: 0 us -> 120 us
  blocking collectives: 73 us -> 5.85 us
  matrix products: 24.5 us -> 7.8 us
    all_gather x5 -> x0, waiting for transfers between devices: 146 us -> none  [the longest x1 45.9 us: shards(): lax.all_gather(w_conv_gate, 'sp', axis=0, tiled=True)]
    pallas_call x0 -> x1, Pallas kernels: none -> 120 us  [gathered(): pl.pallas_call(functools.partial(gather_kernel, count), out_shape=(shape(...]
    all_gather x2 -> x0, blocking collectives: 67 us -> none  [the longest x1 34.2 us: shards(): lax.all_gather(w_key, 'sp', axis=0, tiled=True)]
    dot_general x5 -> x0, matrix products: 12 us -> none  [shards(): jnp.dot(normed, piece, preferred_element_type=jnp.float32)]
  transfers between devices with their start and end apart: 9 -> 4, of which waited for: 5 -> 1; matrix products, arithmetic and copies ran while one was open for 10% -> 7% of each run, Pallas kernels for 0% -> 0%
where the time goes in v1:
time: 201 us
  Pallas kernels  120 us (60%)
  waiting for transfers between devices  30.4 us (15%)
  between operations  14.4 us (7%)
  starting transfers between devices  10 us (5%)
  matrix products  7.8 us (4%)
  local copies, waits for them, and re-layouts  6.58 us (3%)
  other arithmetic  6.2 us (3%)
  blocking collectives  5.85 us (3%)
    pallas_call x1, Pallas kernels, gathered(): pl.pallas_call(functools.partial(gather_kernel, count), out_shape=(shape(...  120 us
    reduce_scatter x1, waiting for transfers between devices, shards(): lax.psum_scatter((jnp.dot(conv_branch, cols_conv, preferred_element_type=...  30.4 us
    ppermute x3, starting transfers between devices, shifted(): lax.ppermute(value, axis, [(source, source + steps) for source in range(i...  10 us
    psum x1, blocking collectives, shards(): total_first, total_second = lax.psum((sum_first, sum_second), 'tp')  5.85 us
    reduce_sum x1, other arithmetic, shards(): sum_first = jnp.sum(conv_out, axis=-1)  5.05 us
  transfers between devices with their start and end apart: 4, of which 1 were waited for; matrix products, arithmetic and copies ran while one was open for 7% of the time, Pallas kernels for 0%

profile of v1, /device:TPU:0, one launch (start us, length us, event | category | flops | bytes accessed | tf_op | source)
XLA Modules:
  0.0 201.0 jit_solution(7956978053964063018)
XLA Ops:
  7.2 1.3 reshape.190.norm_gain
  8.5 119.8 %gather_project.1 = (bf16[512,512]{1,0:T(8,128)(2,1)}, bf16[512,512]{1,0:T(8,128)(2,1)}, bf16[512,128]{1,0:T(8,128)(2,1)}, bf16[512,128]{1,0:T(8,128)(2,1)}, bf1...) custom-call(bf16[512,2048]{1,0:T(8,128)(2,1)} %tokens.1, bf16[1,2048]{1,0:T(2,128)(2,1)} %reshape.190.norm_gain, ...), custom_call_target="tpu_custom_call" | custom-call | tf_op jit(solution)/shard_map/gather_project/pallas_call | solution.py:263
  128.3 1.1 copy.22
  129.4 0.3 multiply_cosine_fusion
  129.8 3.2 %collective-permute-start.2 = (bf16[128,2,64]{0,2,1:T(8,128)(2,1)S(1)}, bf16[128,2,64]{0,2,1:T(8,128)(2,1)S(1)}, u32[]{:S(2)}, u32[]{:S(2)}) collective-permute-start(bf16[128,2,64]{0,2,1:T(8,128)(2,1)S(1)} %pad_maximum_fusion.3), channel_id=1, source_target_pairs={{0,4},{4,8},{8,12},{12,16},{16,20},{20,24},{24,28},{1,5},{5,9},{9,... | collective-permute-start | bytes 98312 | tf_op jit(solution)/shard_map/ppermute | solution.py:25
  133.0 0.8 slice.291
  133.8 3.4 %collective-permute-start.1 = (bf16[128,2,64]{0,2,1:T(8,128)(2,1)S(1)}, bf16[128,2,64]{0,2,1:T(8,128)(2,1)S(1)}, u32[]{:S(2)}, u32[]{:S(2)}) collective-permute-start(bf16[128,2,64]{0,2,1:T(8,128)(2,1)S(1)} %bitcast.107), channel_id=1, source_target_pairs={{0,4},{4,8},{8,12},{12,16},{16,20},{20,24},{24,28},{1,5},{5,9},{9,... | collective-permute-start | bytes 98312 | tf_op jit(solution)/shard_map/ppermute | solution.py:25
  137.3 0.8 slice.229
  138.0 3.4 %collective-permute-start = (bf16[30,512]{1,0:T(8,128)(2,1)S(1)}, bf16[30,512]{1,0:T(8,128)(2,1)S(1)}, u32[]{:S(2)}, u32[]{:S(2)}) collective-permute-start(bf16[30,512]{1,0:T(8,128)(2,1)S(1)} %slice.229), channel_id=1, source_target_pairs={{0,4},{4,8},{8,12},{12,16},{16,20},{20,24},{24,28},{1,5},{5,9},{9,... | collective-permute-start | bytes 92168 | tf_op jit(solution)/shard_map/ppermute | solution.py:25
  141.5 1.3 copy.26
  142.8 0.2 subtract_convert_fusion
  143.1 0.2 broadcast_and_fusion
  143.5 0.1 reshape.198
  144.0 0.1 copy.21
  144.1 0.2 maximum_convert_fusion
  144.3 5.1 %fusion.72 = (f32[512]{0:T(512)S(1)}, f32[512]{0:T(512)S(1)}, f32[512,512]{1,0:T(8,128)S(1)}) fusion(f32[542,512]{1,0:T(8,128)S(1)} %maximum_convert_fusion, f32[512]{0:T(512)S(1)} %bitcast.138, f32[512]{0:T(512)S(1)} %bitcast.139, f32[512]{0:T(512)S(1)} %bitcast.110, f32[512]{0:T(512)S(1)} %bitcast.111, f32[512]{0:T(512)S(1)} %bitcast.112, ...), kind=kLoop, calls=%fused_computation.131 | loop fusion | flops 16776192 | bytes 33622016 | tf_op jit(solution)/shard_map/reduce_sum | solution.py:368
  149.4 5.8 %all-reduce = (f32[512]{0:T(512)S(1)}, f32[512]{0:T(512)S(1)}) all-reduce(f32[512]{0:T(512)S(1)} %get-tuple-element.15, f32[512]{0:T(512)S(1)} %get-tuple-element.14), channel_id=1, replica_groups=mesh['sp'=8,'tp'=4] {'tp'}, use_global_device_ids=true, to_apply=%region_3.0 | all-reduce | flops 1024 | bytes 8192 | tf_op jit(solution)/shard_map/psum | solution.py:370
  155.2 3.0 %fusion.47 = f32[512,2048]{1,0:T(8,128)S(1)} fusion(bf16[512,2048]{1,0:T(8,128)(2,1)} %get-tuple-element.9, f32[512,512]{1,0:T(8,128)S(1)} %get-tuple-element.18, f32[512]{0:T(512)S(1)} %copy-done.5, f32[512]{0:T(512)S(1)} %get-tuple-element.57, f32[512]{0:T(512)S(1)} %get-tuple-element.56), kind=kOutput, calls=%fused_computation.79 | convolution fusion | flops 1075838976 | bytes 7346176 | tf_op jit(solution)/shard_map/dot_general | solution.py:408
  158.3 1.1 fusion.1
  159.6 0.9 fusion.14
  160.5 0.4 copy.30
  160.9 0.1 copy-done
  161.0 2.7 %add_convert_fusion = bf16[512,2048]{1,0:T(8,128)(2,1)} fusion(f32[512,2048]{1,0:T(8,128)S(1)} %fusion.47, bf16[512,2048]{1,0:T(8,128)(2,1)S(1)} %copy-done, bf16[64,8,4,128]{3,2,1,0:T(4,128)(2,1)S(1)} %bitcast.104), kind=kOutput, calls=%fused_computation.7 | convolution fusion | flops 1075838976 | bytes 8912896 | tf_op jit(solution)/shard_map/dot_general | solution.py:409
  163.8 30.4 %reduce-scatter.2.cloned.1.call-done = bf16[128,2048]{1,0:T(8,128)(2,1)} async-done(((bf16[512,2048]{1,0:T(8,128)(2,1)}), bf16[128,2048]{1,0:T(8,128)(2,1)}) %reduce-scatter.2.cloned.1.call-update) | async-done | bytes 524304 | tf_op jit(solution)/shard_map/reduce_scatter | solution.py:406
  (41 shorter events, 1.0 us)
Async XLA Ops:
  7.2 187.0 %reduce-scatter.2.cloned.1.call-start = ((), (), s32[]{:S(2)}) async-start(), calls=%async_computation.1 | async-start | bytes 2621440 | tf_op jit(solution)/shard_map/reduce_scatter | solution.py:406
  8.5 134.5 %copy-start.3 = (f32[31,512]{1,0:T(8,128)S(1)}, f32[31,512]{1,0:T(8,128)}, u32[]{:S(2)}) copy-start(f32[31,512]{1,0:T(8,128)} %param.19) | copy-start | bytes 190468
  128.3 15.1 %copy-start.1 = (bf16[512,128]{1,0:T(8,128)(2,1)S(1)}, bf16[512,128]{1,0:T(8,128)(2,1)}, u32[]{:S(2)}) copy-start(bf16[512,128]{1,0:T(8,128)(2,1)} %get-tuple-element.10) | copy-start | bytes 393220
  128.3 15.6 %copy-start.6 = (f32[8]{0:T(128)S(1)}, f32[8]{0:T(128)}, u32[]{:S(2)}) copy-start(f32[8]{0:T(128)} %param.21) | copy-start | bytes 100
  128.3 15.8 %copy-start.2 = (bf16[512,512]{1,0:T(8,128)(2,1)S(1)}, bf16[512,512]{1,0:T(8,128)(2,1)}, u32[]{:S(2)}) copy-start(bf16[512,512]{1,0:T(8,128)(2,1)} %get-tuple-element.8) | copy-start | bytes 1572868
  129.8 28.5 %collective-permute-start.2 = (bf16[128,2,64]{0,2,1:T(8,128)(2,1)S(1)}, bf16[128,2,64]{0,2,1:T(8,128)(2,1)S(1)}, u32[]{:S(2)}, u32[]{:S(2)}) collective-permute-start(bf16[128,2,64]{0,2,1:T(8,128)(2,1)S(1)} %pad_maximum_fusion.3), channel_id=1, source_target_pairs={{0,4},{4,8},{8,12},{12,16},{16,20},{20,24},{24,28},{1,5},{5,9},{9,... | collective-permute-start | bytes 98312 | tf_op jit(solution)/shard_map/ppermute | solution.py:25
  133.8 25.7 %collective-permute-start.1 = (bf16[128,2,64]{0,2,1:T(8,128)(2,1)S(1)}, bf16[128,2,64]{0,2,1:T(8,128)(2,1)S(1)}, u32[]{:S(2)}, u32[]{:S(2)}) collective-permute-start(bf16[128,2,64]{0,2,1:T(8,128)(2,1)S(1)} %bitcast.107), channel_id=1, source_target_pairs={{0,4},{4,8},{8,12},{12,16},{16,20},{20,24},{24,28},{1,5},{5,9},{9,... | collective-permute-start | bytes 98312 | tf_op jit(solution)/shard_map/ppermute | solution.py:25
  138.0 6.1 %collective-permute-start = (bf16[30,512]{1,0:T(8,128)(2,1)S(1)}, bf16[30,512]{1,0:T(8,128)(2,1)S(1)}, u32[]{:S(2)}, u32[]{:S(2)}) collective-permute-start(bf16[30,512]{1,0:T(8,128)(2,1)S(1)} %slice.229), channel_id=1, source_target_pairs={{0,4},{4,8},{8,12},{12,16},{16,20},{20,24},{24,28},{1,5},{5,9},{9,... | collective-permute-start | bytes 92168 | tf_op jit(solution)/shard_map/ppermute | solution.py:25
  144.3 10.9 %copy-start.5 = (f32[512]{0:T(512)S(1)}, f32[512]{0:T(512)}, u32[]{:S(2)}) copy-start(f32[512]{0:T(512)} %param.20) | copy-start | bytes 6148
  159.4 1.6 copy-start
  159.5 4.2 %copy-start.4 = (f32[4,2,4,128]{3,2,1,0:T(4,128)}, f32[4,2,4,128]{3,2,1,0:T(4,128)S(1)}, u32[]{:S(2)}) copy-start(f32[4,2,4,128]{3,2,1,0:T(4,128)S(1)} %add_log_fusion) | copy-start | bytes 49156
Sparse Core Ops, SparseCore 0:
  163.9 30.1 reduce-scatter.1

commit v2 on v1

--- a/solution.py
+++ b/solution.py
@@ -104,21 +104,9 @@
                         self.copy(phase, way, piece, step).wait_send()
 
 
-def run_phase(ring, phase, work):
-    steps = ring.count - 1
-    done = 0
-    for step in range(steps):
-        upto = (step + 1) * len(work) // steps
-        for item in work[done:upto]:
-            item()
-        done = upto
-        ring.advance(phase, step)
-        if step == steps - 2 and phase + 1 < len(ring.phases):
-            ring.begin(phase + 1)
-
-
-def gather_kernel(
+def layer_kernel(
     count,
+    splits,
     tokens,
     norm_gain,
     w_conv_value,
@@ -126,29 +114,58 @@
     w_query,
     w_key,
     w_value,
+    taps,
+    ln_gain,
+    sinks,
     out_conv,
     out_attn,
-    glu_out,
-    query_out,
-    key_out,
-    value_out,
-    full_conv,
-    full_attn,
+    cosine,
+    sine,
+    mixed_out,
+    logs_out,
     normed,
     full_cv,
     full_cg,
     full_q,
     full_k,
     full_v,
+    full_conv,
+    full_attn,
+    query,
+    key_rows,
+    value_rows,
+    attn,
+    extended,
+    glu_tail,
+    glu_head,
+    conv,
+    first,
+    second,
+    stats,
+    stats_in,
+    branch,
+    share,
+    share_in,
     send_sem,
     recv_sem,
     own_sem,
+    halo_send,
+    halo_recv,
+    stat_send,
+    stat_recv,
+    part_send,
+    part_recv,
 ):
-    me = lax.axis_index("sp")
+    me, rank = lax.axis_index("sp"), lax.axis_index("tp")
     depth, wide = w_query.shape
     narrow = w_key.shape[1]
-    long, cols = out_conv.shape
+    cols = out_conv.shape[1]
     rows = tokens.shape[0]
+    lanes = 128
+    span = rows // splits
+    blocks = rows // WINDOW
+    tiles = wide // lanes
+    mesh_id = pl.DeviceIdType.MESH
 
     def by_rows(own, full, low, high):
         return (
@@ -158,12 +175,11 @@
             ],
         )
 
-    def by_cols(own, full, low, high):
+    def by_cols(own, full, way):
+        half = cols // 2
         return (
-            own.at[pl.ds(low, high - low)],
-            lambda who: full.at[
-                pl.ds(low, high - low), pl.ds(pl.multiple_of(who * cols, cols), cols)
-            ],
+            own.at[:, pl.ds(way * half, half)],
+            lambda who: full.at[:, pl.ds(pl.multiple_of(who * cols + way * half, half), half)],
         )
 
     quarter, middle = wide // 4, wide // 2
@@ -180,18 +196,20 @@
             [by_rows(w_conv_value, full_cv, i * middle, (i + 1) * middle) for i in range(2)],
             [by_rows(w_conv_gate, full_cg, i * middle, (i + 1) * middle) for i in range(2)],
         ),
-        (
-            [by_cols(out_conv, full_conv, i * long // 2, (i + 1) * long // 2) for i in range(2)],
-            [by_cols(out_attn, full_attn, i * long // 2, (i + 1) * long // 2) for i in range(2)],
+        tuple(
+            [by_cols(out_conv, full_conv, way), by_cols(out_attn, full_attn, way)]
+            for way in range(2)
         ),
     )
     ring = Ring(count, phases, send_sem, recv_sem)
+    after, before = lax.rem(me + 1, count), lax.rem(me + count - 1, count)
     barrier = pltpu.get_barrier_semaphore()
-    for peer in ring.peers:
-        pl.semaphore_signal(
-            barrier, inc=1, device_id={"sp": peer}, device_id_type=pl.DeviceIdType.MESH
-        )
-    pl.semaphore_wait(barrier, 2)
+    for peer in ring.peers + (after, before):
+        pl.semaphore_signal(barrier, inc=1, device_id={"sp": peer}, device_id_type=mesh_id)
+    others = [lax.rem(rank + o, splits) for o in range(1, splits)]
+    for peer in others:
+        pl.semaphore_signal(barrier, inc=1, device_id={"tp": peer}, device_id_type=mesh_id)
+    pl.semaphore_wait(barrier, 4 + len(others))
     ring.begin(0)
 
     mine = pl.ds(pl.multiple_of(me * depth, depth), depth)
@@ -213,6 +231,23 @@
     for item in local:
         item.start()
 
+    def forward(source, target, number):
+        return pltpu.make_async_remote_copy(
+            src_ref=source,
+            dst_ref=target,
+            send_sem=halo_send.at[number],
+            recv_sem=halo_recv.at[number],
+            device_id={"sp": after},
+            device_id_type=mesh_id,
+        )
+
+    tail, head = pl.ds(rows, WINDOW), pl.ds(0, WINDOW)
+    halos = (
+        forward(key_rows.at[tail], key_rows.at[head], 0),
+        forward(value_rows.at[tail], value_rows.at[head], 1),
+        forward(glu_tail, glu_head, 2),
+    )
+
     def norm(part):
         take = pl.ds(part * 64, 64)
         x = tokens[take, :].astype(jnp.float32)
@@ -220,71 +255,325 @@
         normed[take, :] = (x * scale * norm_gain[...].astype(jnp.float32)).astype(jnp.bfloat16)
 
     def product(take, full):
-        return jnp.dot(normed[take, :], full[...], preferred_element_type=jnp.float32).astype(
-            jnp.bfloat16
-        )
+        return (
+            jnp.dot(normed[take, :], full[...], preferred_element_type=jnp.float32)
+            .astype(jnp.bfloat16)
+            .astype(jnp.float32)
+        )
+
+    def turned(x, take):
+        lane = lax.broadcasted_iota(jnp.int32, x.shape, 1)
+        swapped = jnp.where(
+            lane % HEAD_DIM < HEAD_DIM // 2,
+            pltpu.roll(x, lanes - HEAD_DIM // 2, 1),
+            pltpu.roll(x, HEAD_DIM // 2, 1),
+        )
+        return (x * cosine[take, :] + swapped * sine[take, :]).astype(jnp.bfloat16)
 
     def attention_side(part):
-        take = pl.ds(part * 128, 128)
-        query_out[take, :] = product(take, full_q)
-        key_out[take, :] = product(take, full_k)
-        value_out[take, :] = product(take, full_v)
+        take = pl.ds(part * WINDOW, WINDOW)
+        put = pl.ds((part + 1) * WINDOW, WINDOW)
+        q = product(take, full_q)
+        for tile in range(tiles):
+            query[take, pl.ds(tile * lanes, lanes)] = turned(
+                q[:, tile * lanes : (tile + 1) * lanes], take
+            )
+        key_rows[put, :] = turned(product(take, full_k), take)
+        value_rows[put, :] = product(take, full_v).astype(jnp.bfloat16)
+
+    def attend(part):
+        take = pl.ds(part * WINDOW, WINDOW)
+        window = pl.ds(part * WINDOW, 2 * WINDOW)
+        low = lax.broadcasted_iota(jnp.int32, (2 * WINDOW, lanes), 1) < HEAD_DIM
+        low_q = lax.broadcasted_iota(jnp.int32, (WINDOW, lanes), 1) < HEAD_DIM
+        keys = key_rows[window, :].astype(jnp.float32)
+        values = value_rows[window, :].astype(jnp.float32)
+        keys_turned, values_turned = pltpu.roll(keys, HEAD_DIM, 1), pltpu.roll(values, HEAD_DIM, 1)
+        group = wide // narrow
+        shape = (group * WINDOW, 2 * WINDOW)
+        row = lax.broadcasted_iota(jnp.int32, shape, 0) % WINDOW
+        col = lax.broadcasted_iota(jnp.int32, shape, 1)
+        start = me * rows + (part - 1) * WINDOW
+        allowed = (col > row) & (col <= row + WINDOW) & (start + col >= 0)
+        lane = lax.broadcasted_iota(jnp.int32, (WINDOW, lanes), 1)
+        totals = jnp.exp(sinks[...]) + jnp.zeros((WINDOW, lanes), jnp.float32)
+        all_scores = []
+        for head in range(2):
+            two = jnp.where(low if head == 0 else ~low, keys, keys_turned).astype(jnp.bfloat16)
+            stacked = []
+            for pair in range(group // 2):
+                tile = head * (group // 2) + pair
+                q = query[take, pl.ds(tile * lanes, lanes)].astype(jnp.float32)
+                stacked += [jnp.where(low_q, q, 0.0), jnp.where(low_q, 0.0, q)]
+            q_all = jnp.concatenate(stacked, axis=0).astype(jnp.bfloat16)
+            scores = lax.dot_general(
+                q_all, two, (((1,), (1,)), ((), ())), preferred_element_type=jnp.float32
+            ) * HEAD_DIM ** (-0.5)
+            all_scores.append(scores)
+            sums = jnp.sum(jnp.where(allowed, jnp.exp(scores), 0.0), axis=-1, keepdims=True)
+            for i in range(group):
+                totals = totals + jnp.where(
+                    lane == head * group + i, sums[i * WINDOW : (i + 1) * WINDOW], 0.0
+                )
+        logs = jnp.log(totals)
+        logs_out[:, pl.ds(part * WINDOW, WINDOW)] = logs.T[: logs_out.shape[0]]
+        for head in range(2):
+            two = jnp.where(low if head == 0 else ~low, values, values_turned).astype(jnp.bfloat16)
+            level = jnp.concatenate(
+                [logs[:, head * group + i : head * group + i + 1] for i in range(group)], axis=0
+            )
+            weights = jnp.where(allowed, jnp.exp(all_scores[head] - level), 0.0)
+            got = jnp.dot(weights.astype(jnp.bfloat16), two, preferred_element_type=jnp.float32)
+            for pair in range(group // 2):
+                tile = head * (group // 2) + pair
+                one = got[2 * pair * WINDOW : (2 * pair + 1) * WINDOW]
+                other = got[(2 * pair + 1) * WINDOW : (2 * pair + 2) * WINDOW]
+                attn[take, pl.ds(tile * lanes, lanes)] = jnp.where(low_q, one, other).astype(
+                    jnp.bfloat16
+                )
+
+    edge = glu_tail.shape[0]
 
     def conv_side(part):
-        take = pl.ds(part * 128, 128)
-        value = product(take, full_cv).astype(jnp.float32)
-        gate = product(take, full_cg).astype(jnp.float32)
-        glu_out[take, :] = (value * jax.nn.sigmoid(gate)).astype(jnp.bfloat16)
-
-    run_phase(ring, 0, [functools.partial(norm, i) for i in range(rows // 64)])
+        take = pl.ds(part * WINDOW, WINDOW)
+        glu = (product(take, full_cv) * jax.nn.sigmoid(product(take, full_cg))).astype(jnp.bfloat16)
+        if part == blocks - 1:
+            glu_tail[...] = glu[WINDOW - edge :]
+        glu = glu.astype(jnp.float32)
+        for tile in range(tiles):
+            extended[tile, pl.ds(edge + part * WINDOW, WINDOW), :] = glu[
+                :, tile * lanes : (tile + 1) * lanes
+            ]
+
+    def take_halo():
+        halos[2].wait_recv()
+        for tile in range(tiles):
+            got = glu_head[:, pl.ds(tile * lanes, lanes)].astype(jnp.float32)
+            extended[tile, pl.ds(0, edge), :] = jnp.where(me > 0, got, 0.0)
+
+    def convolve(tile):
+        reach = taps.shape[0]
+        block = 64
+
+        @pl.loop(0, rows // block)
+        def _(part):
+            base = pl.multiple_of(part * block, block)
+            total = jnp.zeros((block, lanes), jnp.float32)
+            for j in range(reach):
+                total = total + taps[pl.ds(j, 1), pl.ds(tile * lanes, lanes)] * extended[
+                    tile, pl.ds(base + (edge - reach + 1 + j), block), :
+                ]
+            take = pl.ds(base, block)
+            conv[tile, take, :] = total
+            if tile == 0:
+                first[take, :] = total
+                second[take, :] = total * total
+            else:
+                first[take, :] = first[take, :] + total
+                second[take, :] = second[take, :] + total * total
+
+    def stat_copy(o):
+        return pltpu.make_async_remote_copy(
+            src_ref=stats,
+            dst_ref=stats_in.at[o],
+            send_sem=stat_send.at[o],
+            recv_sem=stat_recv.at[o],
+            device_id={"tp": others[o]},
+            device_id_type=mesh_id,
+        )
+
+    def send_stats():
+        lane = lax.broadcasted_iota(jnp.int32, (WINDOW, lanes), 1)
+        mat = jnp.zeros((WINDOW, lanes), jnp.float32)
+        for part in range(blocks):
+            take = pl.ds(part * WINDOW, WINDOW)
+            mat = jnp.where(lane == 2 * part, jnp.sum(first[take, :], -1, keepdims=True), mat)
+            mat = jnp.where(lane == 2 * part + 1, jnp.sum(second[take, :], -1, keepdims=True), mat)
+        stats[...] = mat
+        for o in range(splits - 1):
+            stat_copy(o).start()
+
+    def finish_conv():
+        total = stats[...]
+        for o in range(splits - 1):
+            stat_copy(o).wait_recv()
+            total = total + stats_in[o]
+        total = total / CONV_CH
+        for part in range(blocks):
+            take = pl.ds(part * WINDOW, WINDOW)
+            mean = total[:, 2 * part : 2 * part + 1]
+            scale = lax.rsqrt(total[:, 2 * part + 1 : 2 * part + 2] - mean * mean + CHANNEL_EPS)
+            for tile in range(tiles):
+                at = pl.ds(tile * lanes, lanes)
+                value = (conv[tile, take, :] - mean) * scale * ln_gain[:, at]
+                branch[take, at] = (value * jax.nn.sigmoid(value)).astype(jnp.bfloat16)
+
+    def part_copy(way, step, o):
+        half = cols // 2
+        at = pl.ds(pl.multiple_of(ring.owner(way, step) * cols + way * half, half), half)
+        return pltpu.make_async_remote_copy(
+            src_ref=share.at[pl.ds(pl.multiple_of(others[o] * span, span), span), at],
+            dst_ref=share_in.at[o, :, at],
+            send_sem=part_send.at[way, step, o],
+            recv_sem=part_recv.at[way, step, o],
+            device_id={"tp": others[o]},
+            device_id_type=mesh_id,
+        )
+
+    def project_out(step):
+        half = cols // 2
+        for way in range(2):
+            at = pl.ds(pl.multiple_of(ring.owner(way, step) * cols + way * half, half), half)
+            share[:, at] = (
+                jnp.dot(branch[...], full_conv[:, at], preferred_element_type=jnp.float32)
+                + jnp.dot(attn[...], full_attn[:, at], preferred_element_type=jnp.float32)
+            ).astype(jnp.bfloat16)
+        for way in range(2):
+            for o in range(splits - 1):
+                part_copy(way, step, o).start()
+
+    def run(phase, plan):
+        for step in range(count - 1):
+            for item in plan[step] if step < len(plan) else ():
+                item()
+            ring.advance(phase, step)
+            if step == count - 3 and phase + 1 < len(phases):
+                ring.begin(phase + 1)
+
+    each = functools.partial
+
+    def spread(items, steps):
+        return [
+            items[i * len(items) // steps : (i + 1) * len(items) // steps] for i in range(steps)
+        ]
+
+    run(0, spread([each(norm, i) for i in range(rows // 64)], count - 1))
     for item in local:
         item.wait()
-    run_phase(ring, 1, [functools.partial(attention_side, i) for i in range(rows // 128)])
-    run_phase(ring, 2, [functools.partial(conv_side, i) for i in range(rows // 128)])
+
+    def send_rows():
+        halos[0].start()
+        halos[1].start()
+
+    def take_rows():
+        halos[0].wait_recv()
+        halos[1].wait_recv()
+
+    sides = [each(attention_side, i) for i in range(blocks)]
+    sides.append(send_rows)
+    sides += [each(attend, i) for i in range(1, blocks)]
+    sides += [take_rows, each(attend, 0)]
+    run(1, spread(sides, count - 1))
+    opening = [each(conv_side, i) for i in range(blocks)] + [halos[2].start]
+    middle_work = [take_halo] + [each(convolve, i) for i in range(tiles)] + [send_stats]
+    plan = [opening, middle_work, [finish_conv]]
+    plan.append([each(project_out, i) for i in range(4)])
+    plan += [[each(project_out, i)] for i in range(4, count - 1)]
+    plan = plan if count > 4 else [opening + middle_work + [finish_conv]]
+    run(2, plan)
+    for step in range(count - 1 if count > 4 else 0, count):
+        project_out(step)
     ring.drain()
-
-
-def fits(count, shape_in, shape_out, rows):
-    tiled = shape_in[0] % 128 == 0 and shape_in[1] % 512 == 0 and shape_out[1] % 128 == 0
-    return tiled and rows % 128 == 0 and count % 2 == 0 and count > 3
-
-
-def gathered(
-    tokens, norm_gain, w_conv_value, w_conv_gate, w_query, w_key, w_value, out_conv, out_attn
+    for halo in halos:
+        halo.wait_send()
+    for o in range(splits - 1):
+        stat_copy(o).wait_send()
+    for step in range(count):
+        for way in range(2):
+            for o in range(splits - 1):
+                part_copy(way, step, o).wait()
+    total = share[pl.ds(pl.multiple_of(rank * span, span), span), :].astype(jnp.float32)
+    for o in range(splits - 1):
+        total = total + share_in[o].astype(jnp.float32)
+    mixed_out[...] = total.astype(jnp.bfloat16)
+
+
+def fits(count, splits, tokens, w_query, w_key, out_conv):
+    rows, width = tokens.shape
+    depth, wide = w_query.shape
+    if depth % 128 or wide % 512 or out_conv.shape[1] % 256 or rows % (128 * splits):
+        return False
+    if w_key.shape[1] != 2 * HEAD_DIM or wide != 4 * w_key.shape[1] or rows > 64 * 128:
+        return False
+    return count % 2 == 0 and 3 < count <= 16 and splits > 1
+
+
+def one_kernel(
+    tokens,
+    norm_gain,
+    w_conv_value,
+    w_conv_gate,
+    w_query,
+    w_key,
+    w_value,
+    conv_taps,
+    ln_gain,
+    sinks,
+    out_conv,
+    out_attn,
 ):
-    count = lax.axis_size("sp")
+    count, splits = lax.axis_size("sp"), lax.axis_size("tp")
     rows, width = tokens.shape
     wide, narrow = w_query.shape[1], w_key.shape[1]
     long = out_conv.shape[0]
+    full_cols = count * out_conv.shape[1]
+    tiles = wide // 128
+    edge = 32
+    span = rows // splits
+    half_dim = HEAD_DIM // 2
+    inverse = ROPE_BASE ** (-jnp.arange(half_dim, dtype=jnp.float32) / half_dim)
+    positions = lax.axis_index("sp") * rows + jnp.arange(rows, dtype=jnp.int32)
+    angles = positions.astype(jnp.float32)[:, None] * jnp.tile(inverse, 4)[None, :]
+    sign = jnp.tile(jnp.repeat(jnp.array([-1.0, 1.0], jnp.float32), half_dim), 2)
+    cosine, sine = jnp.cos(angles), jnp.sin(angles) * sign[None, :]
     vmem = pl.BlockSpec(memory_space=pltpu.VMEM)
-    shape = lambda *dims: jax.ShapeDtypeStruct(dims, jnp.bfloat16)
-    scratch = lambda *dims: pltpu.VMEM(dims, jnp.bfloat16)
-    pieces = 7
+    low = lambda *dims: pltpu.VMEM(dims, jnp.bfloat16)
+    high = lambda *dims: pltpu.VMEM(dims, jnp.float32)
+    dma = lambda *dims: pltpu.SemaphoreType.DMA(dims)
     return pl.pallas_call(
-        functools.partial(gather_kernel, count),
+        functools.partial(layer_kernel, count, splits),
         out_shape=(
-            shape(rows, w_conv_value.shape[1]),
-            shape(rows, wide),
-            shape(rows, narrow),
-            shape(rows, narrow),
-            shape(long, count * out_conv.shape[1]),
-            shape(out_attn.shape[0], count * out_attn.shape[1]),
+            jax.ShapeDtypeStruct((span, full_cols), jnp.bfloat16),
+            jax.ShapeDtypeStruct((wide // HEAD_DIM, rows), jnp.float32),
         ),
-        in_specs=[vmem] * 9,
-        out_specs=(vmem,) * 6,
+        in_specs=[vmem] * 14,
+        out_specs=(vmem,) * 2,
         scratch_shapes=[
-            scratch(rows, width),
-            scratch(width, w_conv_value.shape[1]),
-            scratch(width, w_conv_gate.shape[1]),
-            scratch(width, wide),
-            scratch(width, narrow),
-            scratch(width, narrow),
-            pltpu.SemaphoreType.DMA((2, pieces, count - 1)),
-            pltpu.SemaphoreType.DMA((2, pieces, count - 1)),
-            pltpu.SemaphoreType.DMA((7,)),
+            low(rows, width),
+            low(width, wide),
+            low(width, wide),
+            low(width, wide),
+            low(width, narrow),
+            low(width, narrow),
+            low(long, full_cols),
+            low(long, full_cols),
+            low(rows, wide),
+            low(rows + WINDOW, narrow),
+            low(rows + WINDOW, narrow),
+            low(rows, wide),
+            high(tiles, rows + edge, 128),
+            low(edge, wide),
+            low(edge, wide),
+            high(tiles, rows, 128),
+            high(rows, 128),
+            high(rows, 128),
+            high(128, 128),
+            high(splits - 1, 128, 128),
+            low(rows, wide),
+            low(rows, full_cols),
+            low(splits - 1, span, full_cols),
+            dma(2, 7, count - 1),
+            dma(2, 7, count - 1),
+            dma(7),
+            dma(3),
+            dma(3),
+            dma(splits - 1),
+            dma(splits - 1),
+            dma(2, count, splits - 1),
+            dma(2, count, splits - 1),
         ],
         compiler_params=pltpu.CompilerParams(collective_id=0, has_side_effects=True),
-        name="gather_project",
+        name="layer",
     )(
         tokens,
         norm_gain.reshape(1, width),
@@ -293,8 +582,13 @@
         w_query,
         w_key,
         w_value,
+        conv_taps,
+        ln_gain.reshape(1, -1),
+        jnp.pad(sinks, (0, 128 - sinks.shape[0])).reshape(1, 128),
         out_conv,
         out_attn,
+        cosine,
+        sine,
     )
 
 
@@ -343,8 +637,22 @@
     out_attn,
 ):
     row_count = tokens.shape[0]
-    whole = fits(lax.axis_size("sp"), w_query.shape, out_conv.shape, row_count)
-    glu, query_raw, key_raw, value_rows, cols_conv, cols_attn = (gathered if whole else plain)(
+    if fits(lax.axis_size("sp"), lax.axis_size("tp"), tokens, w_query, w_key, out_conv):
+        return one_kernel(
+            tokens,
+            norm_gain,
+            w_conv_value,
+            w_conv_gate,
+            w_query,
+            w_key,
+            w_value,
+            conv_taps,
+            ln_gain,
+            sinks,
+            out_conv,
+            out_attn,
+        )
+    glu, query_raw, key_raw, value_rows, cols_conv, cols_attn = plain(
         tokens, norm_gain, w_conv_value, w_conv_gate, w_query, w_key, w_value, out_conv, out_attn
     )
     offset = lax.axis_index("sp") * row_count

time: 201 us -> 137 us (0.68)
  waiting for transfers between devices: 30.4 us -> 0 us
  between operations: 14.4 us -> 0.65 us
  starting transfers between devices: 10 us -> 0 us
  Pallas kernels: 120 us -> 128 us
  matrix products: 7.8 us -> 0 us
  blocking collectives: 5.85 us -> 0 us
  other arithmetic: 6.2 us -> 1.81 us
    reduce_scatter x1 -> x0, waiting for transfers between devices: 30.4 us -> none  [shards(): lax.psum_scatter((jnp.dot(conv_branch, cols_conv, preferred_element_type=...]
    ppermute x3 -> x0, starting transfers between devices: 10 us -> none  [shifted(): lax.ppermute(value, axis, [(source, source + steps) for source in range(i...]
    pallas_call x1, Pallas kernels: 120 us -> 128 us  [one_kernel(): pl.pallas_call(functools.partial(layer_kernel, count, splits), out_shape=...]
    dot_general x4 -> x0, matrix products: 7.8 us -> none  [the longest x1 3.05 us: shards(): jnp.dot(conv_branch, cols_conv, preferred_element_type=jnp.float32)]
    psum x1 -> x0, blocking collectives: 5.85 us -> none  [shards(): total_first, total_second = lax.psum((sum_first, sum_second), 'tp')]
    reduce_sum x1 -> x0, other arithmetic: 5.05 us -> none  [shards(): sum_first = jnp.sum(conv_out, axis=-1)]
    unnamed x14 -> x2, local copies, waits for them, and re-layouts: 0.16 us -> 3.2 us
    convert_element_type x3 -> x0, local copies, waits for them, and re-layouts: 2.73 us -> none  [the longest x2 2.32 us: rotate(): as_float = heads.astype(jnp.float32)]
  transfers between devices with their start and end apart: 4 -> 0, of which waited for: 1 -> 0; matrix products, arithmetic and copies ran while one was open for 7% -> 0% of each run, Pallas kernels for 0% -> 0%
where the time goes in v2:
time: 137 us
  Pallas kernels  128 us (93%)
  local copies, waits for them, and re-layouts  6.72 us (5%)
  other arithmetic  1.81 us (1%)
    pallas_call x1, Pallas kernels, one_kernel(): pl.pallas_call(functools.partial(layer_kernel, count, splits), out_shape=...  128 us
    unnamed x2, local copies, waits for them, and re-layouts  3.2 us

profile of v2, /device:TPU:0, one launch (start us, length us, event | category | flops | bytes accessed | tf_op | source)
XLA Modules:
  0.0 136.8 jit_solution(4701581397437287097)
XLA Ops:
  0.6 1.2 pad_bitcast_fusion.sinks
  1.9 0.7 broadcast_in_dim.4
  2.6 0.1 tile.14
  2.7 0.1 mul.33
  2.8 0.1 mul.30
  2.9 1.3 reshape.27.norm_gain
  4.2 1.8 %fusion = (f32[512,128]{1,0:T(8,128)}, f32[512,128]{1,0:T(8,128)}) fusion(f32[128]{0:T(128)S(1)} %mul.33, f32[128]{0:T(128)S(1)} %mul.30, f32[512]{0:T(512)S(1)} %add_convert_fusion), kind=kLoop, calls=%fused_computation.2 | loop fusion | flops 131072 | bytes 527360 | tf_op jit(solution)/shard_map/mul | solution.py:528
  6.0 127.6 %layer.1 = (bf16[128,2048]{1,0:T(8,128)(2,1)}, f32[8,512]{1,0:T(8,128)}) custom-call(bf16[512,2048]{1,0:T(8,128)(2,1)} %tokens.1, bf16[1,2048]{1,0:T(2,128)(2,1)} %reshape.27.norm_gain, bf16[256,512]{1,0:T(8,128)(2,1)} %w_conv_value.1, bf16[256,512]{1,0:T(8,128)(2,1)} %w_conv_gate.1, bf16[256,512]{1,0:T(8,128)(2,1)} %w_query.1, bf16[256,128]{1,0:T(8,128)(2,1)} %w_key.1, ...), custom_call_target="tpu_custom_call" | custom-call | tf_op jit(solution)/shard_map/layer/pallas_call | solution.py:533
  133.6 1.9 %copy.17 = bf16[128,2048]{1,0:T(8,128)(2,1)} copy(bf16[128,2048]{1,0:T(8,128)(2,1)} %get-tuple-element.6) | data formatting | bytes 1048576
  135.5 1.3 copy.18
  (4 shorter events, 0.0 us)

commit v3 on v2

--- a/solution.py
+++ b/solution.py
@@ -2,6 +2,7 @@
 
 import jax
 import jax.numpy as jnp
+import numpy as np
 from jax import lax
 from jax.experimental import pallas as pl
 from jax.experimental.pallas import tpu as pltpu
@@ -89,12 +90,11 @@
             for way in range(2):
                 self.copy(phase, way, piece, 0).start()
 
-    def advance(self, phase, step):
-        for piece in range(len(self.phases[phase][0])):
-            for way in range(2):
-                self.arrived(phase, way, piece, step)
-                if step + 1 < self.count - 1:
-                    self.copy(phase, way, piece, step + 1).start()
+    def advance(self, phase, step, piece):
+        for way in range(2):
+            self.arrived(phase, way, piece, step)
+            if step + 1 < self.count - 1:
+                self.copy(phase, way, piece, step + 1).start()
 
     def drain(self):
         for phase in range(len(self.phases)):
@@ -119,8 +119,6 @@
     sinks,
     out_conv,
     out_attn,
-    cosine,
-    sine,
     mixed_out,
     logs_out,
     normed,
@@ -155,6 +153,8 @@
     stat_recv,
     part_send,
     part_recv,
+    cosine,
+    sine,
 ):
     me, rank = lax.axis_index("sp"), lax.axis_index("tp")
     depth, wide = w_query.shape
@@ -252,7 +252,21 @@
         take = pl.ds(part * 64, 64)
         x = tokens[take, :].astype(jnp.float32)
         scale = lax.rsqrt(jnp.mean(x * x, axis=-1, keepdims=True) + NORM_EPS)
-        normed[take, :] = (x * scale * norm_gain[...].astype(jnp.float32)).astype(jnp.bfloat16)
+        normed[take, :] = (x * scale * norm_gain[...].astype(jnp.float32)[None, :]).astype(jnp.bfloat16)
+
+    def table(part):
+        take = pl.ds(part * WINDOW, WINDOW)
+        shape = (WINDOW, lanes)
+        half_dim = HEAD_DIM // 2
+        lane = lax.broadcasted_iota(jnp.int32, shape, 1)
+        place = me * rows + part * WINDOW + lax.broadcasted_iota(jnp.int32, shape, 0)
+        inverse = jnp.zeros(shape, jnp.float32)
+        for i in range(half_dim):
+            exact = float(np.float32(ROPE_BASE ** (-i / half_dim)))
+            inverse = jnp.where(lane % half_dim == i, exact, inverse)
+        angles = place.astype(jnp.float32) * inverse
+        cosine[take, :] = jnp.cos(angles)
+        sine[take, :] = jnp.where(lane % HEAD_DIM < half_dim, -jnp.sin(angles), jnp.sin(angles))
 
     def product(take, full):
         return (
@@ -296,7 +310,10 @@
         start = me * rows + (part - 1) * WINDOW
         allowed = (col > row) & (col <= row + WINDOW) & (start + col >= 0)
         lane = lax.broadcasted_iota(jnp.int32, (WINDOW, lanes), 1)
-        totals = jnp.exp(sinks[...]) + jnp.zeros((WINDOW, lanes), jnp.float32)
+        totals = jnp.zeros((WINDOW, lanes), jnp.float32)
+        for i in range(2 * group):
+            totals = jnp.where(lane == i, sinks[i], totals)
+        totals = jnp.exp(totals)
         all_scores = []
         for head in range(2):
             two = jnp.where(low if head == 0 else ~low, keys, keys_turned).astype(jnp.bfloat16)
@@ -434,9 +451,14 @@
 
     def run(phase, plan):
         for step in range(count - 1):
-            for item in plan[step] if step < len(plan) else ():
-                item()
-            ring.advance(phase, step)
+            items = plan[step] if step < len(plan) else ()
+            pieces = len(phases[phase][0])
+            for piece in range(pieces):
+                for item in items[
+                    piece * len(items) // pieces : (piece + 1) * len(items) // pieces
+                ]:
+                    item()
+                ring.advance(phase, step, piece)
             if step == count - 3 and phase + 1 < len(phases):
                 ring.begin(phase + 1)
 
@@ -447,7 +469,8 @@
             items[i * len(items) // steps : (i + 1) * len(items) // steps] for i in range(steps)
         ]
 
-    run(0, spread([each(norm, i) for i in range(rows // 64)], count - 1))
+    opening = [each(norm, i) for i in range(rows // 64)] + [each(table, i) for i in range(blocks)]
+    run(0, spread(opening, count - 1))
     for item in local:
         item.wait()
 
@@ -466,13 +489,17 @@
     run(1, spread(sides, count - 1))
     opening = [each(conv_side, i) for i in range(blocks)] + [halos[2].start]
     middle_work = [take_halo] + [each(convolve, i) for i in range(tiles)] + [send_stats]
-    plan = [opening, middle_work, [finish_conv]]
-    plan.append([each(project_out, i) for i in range(4)])
-    plan += [[each(project_out, i)] for i in range(4, count - 1)]
-    plan = plan if count > 4 else [opening + middle_work + [finish_conv]]
-    run(2, plan)
-    for step in range(count - 1 if count > 4 else 0, count):
-        project_out(step)
+    early = spread(opening + middle_work, 3)
+    late = [finish_conv] + [each(project_out, i) for i in range(count - 1)]
+    if count > 6:
+        tail_work = [late[:3], late[3:6]] + [[item] for item in late[6:]]
+        run(2, early + tail_work)
+        project_out(count - 1)
+    else:
+        run(2, early)
+        for item in late:
+            item()
+        project_out(count - 1)
     ring.drain()
     for halo in halos:
         halo.wait_send()
@@ -520,12 +547,6 @@
     tiles = wide // 128
     edge = 32
     span = rows // splits
-    half_dim = HEAD_DIM // 2
-    inverse = ROPE_BASE ** (-jnp.arange(half_dim, dtype=jnp.float32) / half_dim)
-    positions = lax.axis_index("sp") * rows + jnp.arange(rows, dtype=jnp.int32)
-    angles = positions.astype(jnp.float32)[:, None] * jnp.tile(inverse, 4)[None, :]
-    sign = jnp.tile(jnp.repeat(jnp.array([-1.0, 1.0], jnp.float32), half_dim), 2)
-    cosine, sine = jnp.cos(angles), jnp.sin(angles) * sign[None, :]
     vmem = pl.BlockSpec(memory_space=pltpu.VMEM)
     low = lambda *dims: pltpu.VMEM(dims, jnp.bfloat16)
     high = lambda *dims: pltpu.VMEM(dims, jnp.float32)
@@ -536,7 +557,7 @@
             jax.ShapeDtypeStruct((span, full_cols), jnp.bfloat16),
             jax.ShapeDtypeStruct((wide // HEAD_DIM, rows), jnp.float32),
         ),
-        in_specs=[vmem] * 14,
+        in_specs=[vmem] * 9 + [pl.BlockSpec(memory_space=pltpu.SMEM)] + [vmem] * 2,
         out_specs=(vmem,) * 2,
         scratch_shapes=[
             low(rows, width),
@@ -571,12 +592,14 @@
             dma(splits - 1),
             dma(2, count, splits - 1),
             dma(2, count, splits - 1),
+            high(rows, 128),
+            high(rows, 128),
         ],
         compiler_params=pltpu.CompilerParams(collective_id=0, has_side_effects=True),
         name="layer",
     )(
         tokens,
-        norm_gain.reshape(1, width),
+        norm_gain,
         w_conv_value,
         w_conv_gate,
         w_query,
@@ -584,11 +607,9 @@
         w_value,
         conv_taps,
         ln_gain.reshape(1, -1),
-        jnp.pad(sinks, (0, 128 - sinks.shape[0])).reshape(1, 128),
+        sinks,
         out_conv,
         out_attn,
-        cosine,
-        sine,
     )
 
 

time: 137 us -> 134 us (0.978)
  local copies, waits for them, and re-layouts: 6.72 us -> 3.2 us
  Pallas kernels: 128 us -> 130 us
  other arithmetic: 1.81 us -> 0 us
    reshape x2 -> x0, local copies, waits for them, and re-layouts: 2.52 us -> none  [the longest x1 1.29 us: one_kernel(): norm_gain.reshape(1, width)]
    pallas_call x1, Pallas kernels: 128 us -> 130 us  [one_kernel(): pl.pallas_call(functools.partial(layer_kernel, count, splits), out_shape=...]
    mul x1 -> x0, other arithmetic: 1.8 us -> none  [one_kernel(): cosine, sine = (jnp.cos(angles), jnp.sin(angles) * sign[None, :])]
where the time goes in v3:
time: 134 us; the launch traced here: 133 us
  Pallas kernels  130 us (97%)
  local copies, waits for them, and re-layouts  3.2 us (2%)
    pallas_call x1, Pallas kernels, one_kernel(): pl.pallas_call(functools.partial(layer_kernel, count, splits), out_shape=...  130 us
    unnamed x2, local copies, waits for them, and re-layouts  3.2 us

profile of v3, /device:TPU:0, one launch (start us, length us, event | category | flops | bytes accessed | tf_op | source)
XLA Modules:
  0.0 133.4 jit_solution(2998590623111055476)
XLA Ops:
  0.6 129.5 %layer.1 = (bf16[128,2048]{1,0:T(8,128)(2,1)}, f32[8,512]{1,0:T(8,128)}) custom-call(bf16[512,2048]{1,0:T(8,128)(2,1)} %tokens.1, bf16[2048]{0:T(1024)(128)(2,1)} %norm_gain.1, bf16[256,512]{1,0:T(8,128)(2,1)} %w_conv_value.1, bf16[256,512]{1,0:T(8,128)(2,1)} %w_conv_gate.1, bf16[256,512]{1,0:T(8,128)(2,1)} %w_query.1, bf16[256,128]{1,0:T(8,128)(2,1)} %w_key.1, ...), custom_call_target="tpu_custom_call" | custom-call | tf_op jit(solution)/shard_map/layer/pallas_call | solution.py:554
  130.1 1.9 %copy.16 = bf16[128,2048]{1,0:T(8,128)(2,1)} copy(bf16[128,2048]{1,0:T(8,128)(2,1)} %get-tuple-element.4) | data formatting | bytes 1048576
  132.0 1.3 copy.17
